TPU v7x, 256 devices: a 4x2x16 block of a 4x16x16 slice. The times are simulated.
256 devices in a mesh: grp: 2 (over y), ep: 32 (over z, core), tp: 4 (over x).
Axes of the slice: x: 4, y: 2, z: 16, core: 2. Of those that a mesh axis runs over, the one named last changes fastest.
The devices are a block of a 4x16x16 slice.
Arguments:
- x_in: bfloat16 [4096, 2048], P(('grp', 'ep')), parts along dimension 0, may hold values from -6 to 6
- state: float32 [4096, 96, 128], P(('grp', 'ep'), 'tp'), parts along dimension 0, may hold values from -6 to 6
- routes: int32 [4096, 2], P(('grp', 'ep')), parts along dimension 0, may hold values from 0 to 63, as said below
- w_in: bfloat16 [2048, 1536], P(None, 'tp'), may hold values from -0.125 to 0.125
- decay_rate: float32 [96, 64], P('tp'), may hold values from 0.01 to 1
- frequency: float32 [96, 64], P('tp'), may hold values from 0 to 192
- log_step: float32 [96], P('tp'), may hold values from -3 to 0
- b_in: float32 [96, 16, 128], P('tp'), may hold values from -1.5 to 1.5
- c_out: float32 [96, 16, 128], P('tp'), may hold values from -0.5 to 0.5
- skip: float32 [1536], P('tp'), may hold values from -3 to 3
- w_out: bfloat16 [1536, 2048], P('tp'), may hold values from -0.15625 to 0.15625
- gain_mix: float32 [2048], replicated, may hold values from 0.1 to 1.9
- w_group: bfloat16 [2048, 4], replicated, may hold values from -0.0625 to 0.0625
- w_expert: bfloat16 [2048, 64], replicated, may hold values from -0.0625 to 0.0625
- w_gate: bfloat16 [64, 2048, 1024], P('ep', None, 'tp'), may hold values from -0.125 to 0.125
- w_up: bfloat16 [64, 2048, 1024], P('ep', None, 'tp'), may hold values from -0.125 to 0.125
- w_down: bfloat16 [64, 1024, 2048], P('ep', 'tp'), may hold values from -3 to 3
- gain_moe: float32 [2048], replicated, may hold values from 0.1 to 1.9
Outputs:
- layer_out: bfloat16 [4096, 2048], P(('grp', 'ep')), parts along dimension 0
- new_state: float32 [4096, 96, 128], P(('grp', 'ep'), 'tp'), parts along dimension 0
There are 2 independent parts, one for each index of `grp`. A program takes and returns all parts, laid end to end along the dimension named above; an argument that names none is the same for every part. Nothing has to cross between parts.
Inputs may be any that keep to these rules, and one draw needn't show every extreme that they name: `routes`: each row names two different experts of one group of 16 consecutive expert numbers. Within the rows of one index of ep (aligned blocks of 64 rows) no expert is named by more than 4 rows, and in every block some expert is named by exactly 4 rows.
All inputs are finite; a program needn't handle non-finite values.
Results may differ from a plain program's by a relative error of at most 0.015.
Values may be sent and summed in bfloat16 or wider, within the bound.
A program may use at most 64 MiB of HBM per device.

v0:
```python
import jax
import jax.numpy as jnp
from jax import lax
from jax.sharding import PartitionSpec as P

residual_scale = 8.0**0.25
norm_eps = 1e-05


def sent_to_all(x, axis):
    devices = lax.axis_size(axis)
    return lax.all_to_all(jnp.broadcast_to(x[None], (devices, *x.shape)), axis, 0, 0, tiled=True)


def taken_together(x, axis):
    everything = sent_to_all(x, axis)
    return jnp.sum(everything.astype(jnp.float32), axis=0)


def in_order(parts, dim):
    lengths = list(parts.shape[1:])
    lengths[dim] *= parts.shape[0]
    return jnp.moveaxis(parts, 0, dim).reshape(lengths)


def gather_directly(x, axis, dim):
    parts = sent_to_all(x, axis)
    return in_order(parts, dim)


def split_up(x, dim, devices):
    before, after = (x.shape[:dim], x.shape[dim + 1 :])
    return jnp.moveaxis(x.reshape(*before, devices, -1, *after), dim, 0)


def sent_and_summed(x, axis, dim):
    devices = lax.axis_size(axis)
    parts = lax.all_to_all(split_up(x, dim, devices), axis, 0, 0, tiled=True)
    return jnp.sum(parts.astype(jnp.float32), axis=0)


def normalize(values, gain):
    centre = jnp.mean(values, -1, keepdims=True)
    spread = jnp.mean(jnp.square(values - centre), -1, keepdims=True)
    return (values - centre) * lax.rsqrt(spread + norm_eps) * gain


def s5_advance(mix_input, state, decay_rate, frequency, log_step, b_in, c_out, skip):
    top_precision = lax.Precision.DEFAULT
    entries = decay_rate.shape[-1]
    group_count = decay_rate.shape[0]
    width = b_in.shape[1]
    seq_count = mix_input.shape[0]
    input_rows = mix_input.astype(jnp.float32).reshape(seq_count, group_count, width)
    step_size = jnp.exp(log_step)[:, None]
    lam_real = -decay_rate
    magnitude = jnp.exp(lam_real * step_size)
    angle_dt = frequency * step_size
    bar_real = magnitude * jnp.cos(angle_dt)
    bar_imag = magnitude * jnp.sin(angle_dt)
    minus_real = bar_real - 1.0
    modulus = lam_real * lam_real + frequency * frequency
    ratio_real = (minus_real * lam_real + bar_imag * frequency) / modulus
    ratio_imag = (bar_imag * lam_real - minus_real * frequency) / modulus
    in_real = b_in[..., :entries]
    in_imag = b_in[..., entries:]
    input_matrix_real = ratio_real[:, None, :] * in_real - ratio_imag[:, None, :] * in_imag
    input_matrix_imag = ratio_real[:, None, :] * in_imag + ratio_imag[:, None, :] * in_real
    forcing_real = jnp.einsum(
        "rxf,xfb->rxb", input_rows, input_matrix_real, precision=top_precision
    )
    forcing_imag = jnp.einsum(
        "rxf,xfb->rxb", input_rows, input_matrix_imag, precision=top_precision
    )
    old_real = state[..., :entries]
    old_imag = state[..., entries:]
    following_real = bar_real * old_real - bar_imag * old_imag + forcing_real
    following_imag = bar_real * old_imag + bar_imag * old_real + forcing_imag
    output_real = c_out[..., :entries]
    output_imag = c_out[..., entries:]
    output_matrix = jnp.einsum("lzt,zft->lzf", following_real, output_real, precision=top_precision)
    output_matrix = output_matrix - jnp.einsum(
        "lzt,zft->lzf", following_imag, output_imag, precision=top_precision
    )
    output_matrix = output_matrix + skip.reshape(group_count, width) * input_rows
    activated = jax.nn.gelu(output_matrix).reshape(seq_count, group_count * width)
    return (activated, jnp.concatenate([following_real, following_imag], axis=-1))


def route_weights(normed, routes, w_group, w_expert):
    group_total = w_group.shape[1]
    expert_total = w_expert.shape[1]
    per_group = expert_total // group_total
    group_logit = jnp.dot(normed, w_group, preferred_element_type=jnp.float32)
    group_exp = jnp.exp(group_logit)
    group_prob = group_exp / jnp.sum(group_exp, -1, keepdims=True)
    chosen = routes[:, 0] // per_group
    group_pick = jnp.sum(
        jnp.where(
            chosen[:, None] == jnp.arange(group_total, dtype=jnp.int32)[None, :], group_prob, 0.0
        ),
        -1,
    )
    expert_logit = jnp.dot(normed, w_expert, preferred_element_type=jnp.float32)
    picked = jnp.sum(
        jnp.where(
            routes[:, :, None] == jnp.arange(expert_total, dtype=jnp.int32)[None, None, :],
            expert_logit[:, None, :],
            0.0,
        ),
        -1,
    )
    pair_exp = jnp.exp(picked)
    return pair_exp / jnp.sum(pair_exp, -1, keepdims=True) * group_pick[:, None]


def per_device(
    x_in,
    state,
    routes,
    w_in,
    decay_rate,
    frequency,
    log_step,
    b_in,
    c_out,
    skip,
    w_out,
    gain_mix,
    w_group,
    w_expert,
    w_gate,
    w_up,
    w_down,
    gain_moe,
):
    top_precision = lax.Precision.DEFAULT
    seq_count = x_in.shape[0]
    model_width = x_in.shape[1]
    mix_input = jnp.dot(x_in, w_in, preferred_element_type=jnp.float32).astype(jnp.bfloat16)
    activated, new_state = s5_advance(
        mix_input, state, decay_rate, frequency, log_step, b_in, c_out, skip
    )
    partial_mix = jnp.dot(activated.astype(jnp.bfloat16), w_out, preferred_element_type=jnp.float32)
    mixed = taken_together(partial_mix.astype(jnp.bfloat16), "tp").astype(jnp.float32)
    hidden_state = normalize(residual_scale * x_in.astype(jnp.float32) + mixed, gain_mix)
    hidden_bf = hidden_state.astype(jnp.bfloat16)
    route_weight = route_weights(hidden_bf, routes, w_group, w_expert)
    expert_total = w_expert.shape[1]
    ep_count = lax.axis_size("ep")
    local_experts = w_gate.shape[0]
    capacity = max(2, 4 * seq_count // expert_total)
    total_slots = expert_total * capacity
    hits = (routes[:, :, None] == jnp.arange(expert_total, dtype=jnp.int32)[None, None, :]).astype(
        jnp.int32
    )
    tally = jnp.sum(hits, axis=1)
    prior = jnp.cumsum(tally, axis=0) - tally
    slot_in_block = jnp.sum(prior[:, None, :] * hits, axis=-1)
    target = routes * capacity + slot_in_block
    slot_ids = jnp.arange(total_slots, dtype=jnp.int32)
    matches = target[:, :, None] == slot_ids[None, None, :]
    dispatch_map = jnp.any(slot_ids[:, None, None] == target[None, :, :], axis=-1).astype(
        jnp.bfloat16
    )
    combine_map = jnp.sum(jnp.where(matches, route_weight[:, :, None], 0.0), axis=1)
    buffer = jnp.dot(dispatch_map, hidden_bf, preferred_element_type=jnp.float32).astype(
        jnp.bfloat16
    )
    buffer = buffer.reshape(ep_count, local_experts, capacity, model_width)
    column_width = model_width // lax.axis_size("tp")
    own_columns = lax.dynamic_slice_in_dim(
        buffer, lax.axis_index("tp") * column_width, column_width, 3
    )
    piece = gather_directly(
        lax.all_to_all(own_columns, "ep", split_axis=0, concat_axis=0, tiled=True), "tp", 3
    )
    gate_part = jnp.einsum("njcd,jdf->njcf", piece, w_gate, preferred_element_type=jnp.float32)
    up_part = jnp.einsum("njcd,jdf->njcf", piece, w_up, preferred_element_type=jnp.float32)
    act = (jax.nn.silu(gate_part) * up_part).astype(jnp.bfloat16)
    share = sent_and_summed(
        jnp.einsum("njcf,jfd->njcd", act, w_down, preferred_element_type=jnp.float32).astype(
            jnp.bfloat16
        ),
        "tp",
        3,
    ).astype(jnp.bfloat16)
    returned_rows = lax.all_to_all(share, "ep", split_axis=0, concat_axis=0, tiled=True)
    flat_rows = returned_rows.reshape(total_slots, returned_rows.shape[3])
    moe = jnp.dot(
        combine_map,
        lax.all_gather(flat_rows, "tp", axis=1, tiled=True).astype(jnp.float32),
        precision=top_precision,
    )
    layer_out = normalize(residual_scale * hidden_state + moe, gain_moe).astype(jnp.bfloat16)
    return (layer_out, new_state)


def solution(mesh):
    in_specs = (
        P(("grp", "ep"), None),
        P(("grp", "ep"), "tp", None),
        P(("grp", "ep"), None),
        P(None, "tp"),
        P("tp", None),
        P("tp", None),
        P("tp"),
        P("tp", None, None),
        P("tp", None, None),
        P("tp"),
        P("tp", None),
        P(),
        P(),
        P(),
        P("ep", None, "tp"),
        P("ep", None, "tp"),
        P("ep", "tp", None),
        P(),
    )
    out_specs = (P(("grp", "ep"), None), P(("grp", "ep"), "tp", None))
    return jax.shard_map(
        per_device, mesh=mesh, in_specs=in_specs, out_specs=out_specs, check_vma=False
    )
```

profile of v0, /device:TPU:40, one launch (start us, length us, event | category | flops | bytes accessed | tf_op | source)
XLA Modules:
  0.0 197.4 jit_solution(56538877208457532)
XLA Ops:
  7.2 0.8 exp.20
  8.0 1.9 convolution_convert_fusion.3
  10.9 0.5 fusion.5
  11.4 1.4 fusion.6
  12.9 1.6 fusion.41
  15.3 1.2 broadcast_in_dim.24
  16.4 4.6 %all-to-all-start = ((bf16[4,64,2048]{2,1,0:T(8,128)(2,1)}), bf16[4,64,2048]{2,1,0:T(8,128)(2,1)}, u32[]{:S(2)}, u32[]{:S(2)}) async-start(bf16[4,64,2048]{2,1,0:T(8,128)(2,1)} %broadcast_in_dim.24), calls=%async_computation | async-start | bytes 2097152 | tf_op jit(solution)/shard_map/all_to_all | solution.py:12
  21.5 14.8 %all-to-all-done = bf16[4,64,2048]{2,1,0:T(8,128)(2,1)} async-done(((bf16[4,64,2048]{2,1,0:T(8,128)(2,1)}), bf16[4,64,2048]{2,1,0:T(8,128)(2,1)}, u32[]{:S(2)}, u32[]{:S(2)}) %all-to-all-start) | async-done | bytes 1048608 | tf_op jit(solution)/shard_map/all_to_all | solution.py:12
  36.3 1.4 convert_reduce_fusion
  37.7 1.1 fusion.59
  38.8 1.2 multiply_reduce_fusion.1
  40.0 1.1 fusion.23
  41.2 0.7 copy-done.3
  41.8 1.5 convolution_convert_fusion.1
  43.3 2.3 %reshape.109 = bf16[32,2,4,2048]{3,2,1,0:T(4,128)(2,1)} reshape(bf16[256,2048]{1,0:T(8,128)(2,1)} %convolution_convert_fusion.1) | data formatting | bytes 2097152 | tf_op jit(solution)/shard_map/reshape | solution.py:170
  45.6 1.0 constant_dynamic-slice_fusion
  46.6 46.5 %all_to_all.25 = bf16[32,2,4,512]{3,2,1,0:T(4,128)(2,1)S(1)} all-to-all(bf16[32,2,4,512]{3,2,1,0:T(4,128)(2,1)S(1)} %constant_dynamic-slice_fusion), channel_id=1, replica_groups=mesh['grp'=2,'ep'=32,'tp'=4] {'ep'}, dimensions={0} | all-to-all | bytes 524288 | tf_op jit(solution)/shard_map/all_to_all | solution.py:176
  93.4 18.0 %all_to_all.26 = bf16[4,32,2,4,512]{4,1,3,2,0:T(8,128)(2,1)S(1)} all-to-all(bf16[4,32,2,4,512]{4,1,3,2,0:T(8,128)(2,1)S(1)} %broadcast_in_dim.34), channel_id=1, replica_groups=mesh['grp'=2,'ep'=32,'tp'=4] {'tp'}, dimensions={0} | all-to-all | bytes 2097152 | tf_op jit(solution)/shard_map/all_to_all | solution.py:12
  111.6 1.0 copy-done.1
  112.6 1.2 fusion.7
  113.7 3.8 %convolution_convert_fusion = bf16[2,32,4,2048]{3,1,2,0:T(8,128)(2,1)} fusion(bf16[2,256,2048]{2,1,0:T(8,128)(2,1)S(1)} %copy-done, bf16[32,2,4,2048]{3,0,2,1:T(8,128)(2,1)} %bitcast.85, bf16[2,2048,256]{2,1,0:T(8,128)(2,1)} %param.33, f32[32,2,4,256]{3,0,2,1:T(8,128)} %fusion.7), kind=kOutput, calls=%fused_computation | convolution fusion | flops 537788416 | bytes 6553600 | tf_op jit(solution)/shard_map/njcf,jfd->njcd/dot_general | solution.py:182
  117.5 1.4 copy.95
  118.8 17.5 %all_to_all.27 = bf16[4,32,2,4,512]{4,1,3,2,0:T(8,128)(2,1)} all-to-all(bf16[4,32,2,4,512]{4,1,3,2,0:T(8,128)(2,1)S(1)} %bitcast.88), channel_id=1, replica_groups=mesh['grp'=2,'ep'=32,'tp'=4] {'tp'}, dimensions={0} | all-to-all | bytes 2097152 | tf_op jit(solution)/shard_map/all_to_all | solution.py:38
  136.3 2.2 %reduce_sum.130 = bf16[32,2,4,512]{3,0,2,1:T(8,128)(2,1)} reduce(bf16[4,32,2,4,512]{4,1,3,2,0:T(8,128)(2,1)} %all_to_all.27, bf16[]{:T(256)} %constant.58.clone.1), dimensions={0}, to_apply=%region_12.13 | reduce | flops 393216 | bytes 1310722 | tf_op jit(solution)/shard_map/reduce_sum | solution.py:39
  138.5 1.2 copy.80
  139.7 26.5 %all_to_all.28 = bf16[32,2,4,512]{3,2,1,0:T(4,128)(2,1)} all-to-all(bf16[32,2,4,512]{3,2,1,0:T(4,128)(2,1)S(1)} %copy.80), channel_id=1, replica_groups=mesh['grp'=2,'ep'=32,'tp'=4] {'ep'}, dimensions={0} | all-to-all | bytes 524288 | tf_op jit(solution)/shard_map/all_to_all | solution.py:188
  166.2 1.7 reshape.112
  168.0 1.5 pad_maximum_fusion
  169.5 1.3 copy.81
  171.7 16.1 %all-gather.2.cloned.1.call-done = bf16[256,2048]{1,0:T(8,128)(2,1)} async-done(((bf16[256,512]{1,0:T(8,128)(2,1)}), bf16[256,2048]{1,0:T(8,128)(2,1)}) %all-gather.2.cloned.1.call-update) | async-done | bytes 1048592 | tf_op jit(solution)/shard_map/all_gather | solution.py:192
  187.8 1.7 fusion.62
  189.7 0.8 multiply_convert_fusion
  (64 shorter events, 3.7 us)
Async XLA Ops:
  7.2 106.6 %copy-start = (bf16[2,256,2048]{2,1,0:T(8,128)(2,1)S(1)}, bf16[2,256,2048]{2,1,0:T(8,128)(2,1)}, u32[]{:S(2)}) copy-start(bf16[2,256,2048]{2,1,0:T(8,128)(2,1)} %param.34) | copy-start | bytes 6291460
  7.2 2.9 %copy-start.5 = (f32[64,24,128]{2,1,0:T(8,128)S(1)}, f32[64,24,128]{2,1,0:T(8,128)}, u32[]{:S(2)}) copy-start(f32[64,24,128]{2,1,0:T(8,128)} %param.19) | copy-start | bytes 2359300
  9.9 0.7 copy-start.14
  9.9 0.7 copy-start.15
  9.9 0.9 copy-start.9
  10.9 1.9 copy-start.17
  10.9 2.0 %copy-start.8 = (f32[24,16,128]{2,1,0:T(8,128)S(1)}, f32[24,16,128]{2,1,0:T(8,128)}, u32[]{:S(2)}) copy-start(f32[24,16,128]{2,1,0:T(8,128)} %param.26) | copy-start | bytes 589828
  12.9 2.0 %copy-start.7 = (bf16[384,2048]{1,0:T(8,128)(2,1)S(1)}, bf16[384,2048]{1,0:T(8,128)(2,1)}, u32[]{:S(2)}) copy-start(bf16[384,2048]{1,0:T(8,128)(2,1)} %param.28) | copy-start | bytes 4718596
  15.3 5.8 %copy-start.13 = (s32[64,2]{0,1:T(2,128)S(1)}, s32[64,2]{0,1:T(2,128)}, u32[]{:S(2)}) copy-start(s32[64,2]{0,1:T(2,128)} %param.20) | copy-start | bytes 1540
  16.4 19.8 %all-to-all-start = ((bf16[4,64,2048]{2,1,0:T(8,128)(2,1)}), bf16[4,64,2048]{2,1,0:T(8,128)(2,1)}, u32[]{:S(2)}, u32[]{:S(2)}) async-start(bf16[4,64,2048]{2,1,0:T(8,128)(2,1)} %broadcast_in_dim.24), calls=%async_computation | async-start | bytes 2097152 | tf_op jit(solution)/shard_map/all_to_all | solution.py:12
  21.0 19.0 %copy-start.11 = (f32[2048]{0:T(1024)S(1)}, f32[2048]{0:T(1024)}, u32[]{:S(2)}) copy-start(f32[2048]{0:T(1024)} %param.29) | copy-start | bytes 24580
  21.0 166.7 %all-gather.2.cloned.1.call-start = ((), (), s32[]{:S(2)}) async-start(), calls=%async_computation.5 | async-start | bytes 1310720 | tf_op jit(solution)/shard_map/all_gather | solution.py:192
  41.1 0.7 copy-start.3
  93.4 19.2 %copy-start.6 = (bf16[2,2048,256]{2,1,0:T(8,128)(2,1)S(1)}, bf16[2,2048,256]{2,1,0:T(8,128)(2,1)}, u32[]{:S(2)}) copy-start(bf16[2,2048,256]{2,1,0:T(8,128)(2,1)} %param.32) | copy-start | bytes 6291460
  111.6 1.0 copy-start.1
  168.0 2.9 %copy-start.4 = (bf16[64,2048]{1,0:T(8,128)(2,1)S(1)}, bf16[64,2048]{1,0:T(8,128)(2,1)}, u32[]{:S(2)}) copy-start(bf16[64,2048]{1,0:T(8,128)(2,1)} %copy-done.3) | copy-start | bytes 786436
  168.0 2.9 %copy-start.10 = (bf16[2048,64]{0,1:T(8,128)(2,1)S(1)}, bf16[2048,64]{0,1:T(8,128)(2,1)}, u32[]{:S(2)}) copy-start(bf16[2048,64]{0,1:T(8,128)(2,1)} %param.31) | copy-start | bytes 786436
  168.0 3.3 %copy-start.12 = (bf16[2048,4]{0,1:T(4,128)(2,1)S(1)}, bf16[2048,4]{0,1:T(4,128)(2,1)}, u32[]{:S(2)}) copy-start(bf16[2048,4]{0,1:T(4,128)(2,1)} %param.30) | copy-start | bytes 49156
  169.5 18.3 %copy-start.2 = (bf16[64,2048]{1,0:T(8,128)(2,1)S(1)}, bf16[64,2048]{1,0:T(8,128)(2,1)}, u32[]{:S(2)}) copy-start(bf16[64,2048]{1,0:T(8,128)(2,1)} %param.18) | copy-start | bytes 786436
  170.8 18.8 %copy-start.16 = (f32[2048]{0:T(1024)S(1)}, f32[2048]{0:T(1024)}, u32[]{:S(2)}) copy-start(f32[2048]{0:T(1024)} %param.35) | copy-start | bytes 24580
Sparse Core Ops, SparseCore 0:
  168.1 19.5 all-gather.1
where the time goes:
time: 198 us; the launch traced here: 197 us
  blocking collectives  109 us (55%)
  waiting for transfers between devices  30.9 us (16%)
  matrix products  14.6 us (7%)
  between operations  14.4 us (7%)
  local copies, waits for them, and re-layouts  13.8 us (7%)
  other arithmetic  10.5 us (5%)
  starting transfers between devices  4.58 us (2%)
    all_to_all x1, blocking collectives, per_device(): lax.all_to_all(own_columns, 'ep', split_axis=0, concat_axis=0, tiled=True)  46.5 us
    all_to_all x1, blocking collectives, per_device(): lax.all_to_all(share, 'ep', split_axis=0, concat_axis=0, tiled=True)  26.5 us
    all_to_all x1, blocking collectives, sent_to_all(): lax.all_to_all(jnp.broadcast_to(x[None], (devices, *x.shape)), axis, 0, 0...  18 us
    all_to_all x1, blocking collectives, sent_and_summed(): parts = lax.all_to_all(split_up(x, dim, devices), axis, 0, 0, tiled=True)  17.5 us
    all_gather x1, waiting for transfers between devices, per_device(): lax.all_gather(flat_rows, 'tp', axis=1, tiled=True).astype(jnp.float32)  16.1 us
    all_to_all x1, waiting for transfers between devices, sent_to_all(): lax.all_to_all(jnp.broadcast_to(x[None], (devices, *x.shape)), axis, 0, 0...  14.8 us
    all_to_all x1, starting transfers between devices, sent_to_all(): lax.all_to_all(jnp.broadcast_to(x[None], (devices, *x.shape)), axis, 0, 0...  4.58 us
  transfers between devices with their start and end apart: 2, of which 2 were waited for; matrix products, arithmetic and copies ran while one was open for 2% of the time, Pallas kernels for 0%

commit v1 on v0

--- a/solution.py
+++ b/solution.py
@@ -187,9 +187,13 @@
     ).astype(jnp.bfloat16)
     returned_rows = lax.all_to_all(share, "ep", split_axis=0, concat_axis=0, tiled=True)
     flat_rows = returned_rows.reshape(total_slots, returned_rows.shape[3])
+
+    def wrap_tracks(field, peer_axis):
+        return jnp.concatenate(lax.all_gather(field, peer_axis), axis=1)
+
     moe = jnp.dot(
         combine_map,
-        lax.all_gather(flat_rows, "tp", axis=1, tiled=True).astype(jnp.float32),
+        wrap_tracks(flat_rows, peer_axis="tp").astype(jnp.float32),
         precision=top_precision,
     )
     layer_out = normalize(residual_scale * hidden_state + moe, gain_moe).astype(jnp.bfloat16)

time: 198 us -> 201 us (1.015)
  local copies, waits for them, and re-layouts: 13.8 us -> 16.1 us
    all_gather x0 -> x1, local copies, waits for them, and re-layouts: none -> 2.28 us  [wrap_tracks(): return jnp.concatenate(lax.all_gather(field, peer_axis), axis=1)]
where the time goes in v1:
time: 201 us; the launch traced here: 200 us
  blocking collectives  109 us (54%)
  waiting for transfers between devices  30.9 us (15%)
  local copies, waits for them, and re-layouts  16.1 us (8%)
  matrix products  14.7 us (7%)
  between operations  14.4 us (7%)
  other arithmetic  10.5 us (5%)
  starting transfers between devices  4.58 us (2%)
    all_to_all x1, blocking collectives, per_device(): lax.all_to_all(own_columns, 'ep', split_axis=0, concat_axis=0, tiled=True)  46.5 us
    all_to_all x1, blocking collectives, per_device(): lax.all_to_all(share, 'ep', split_axis=0, concat_axis=0, tiled=True)  26.5 us
    all_to_all x1, blocking collectives, sent_to_all(): lax.all_to_all(jnp.broadcast_to(x[None], (devices, *x.shape)), axis, 0, 0...  18 us
    all_to_all x1, blocking collectives, sent_and_summed(): parts = lax.all_to_all(split_up(x, dim, devices), axis, 0, 0, tiled=True)  17.5 us
    all_gather x1, waiting for transfers between devices, wrap_tracks(): return jnp.concatenate(lax.all_gather(field, peer_axis), axis=1)  16.1 us
    all_to_all x1, waiting for transfers between devices, sent_to_all(): lax.all_to_all(jnp.broadcast_to(x[None], (devices, *x.shape)), axis, 0, 0...  14.8 us
    all_to_all x1, starting transfers between devices, sent_to_all(): lax.all_to_all(jnp.broadcast_to(x[None], (devices, *x.shape)), axis, 0, 0...  4.58 us
  transfers between devices with their start and end apart: 2, of which 2 were waited for; matrix products, arithmetic and copies ran while one was open for 2% of the time, Pallas kernels for 0%

profile of v1, /device:TPU:40, one launch (start us, length us, event | category | flops | bytes accessed | tf_op | source)
XLA Modules:
  0.0 199.8 jit_solution(11680402529090747527)
XLA Ops:
  7.2 0.8 exp.20
  8.0 1.9 convolution_convert_fusion.3
  11.4 1.4 fusion.6
  12.9 1.6 fusion.41
  15.3 1.2 broadcast_in_dim.24
  16.4 4.6 %all-to-all-start = ((bf16[4,64,2048]{2,1,0:T(8,128)(2,1)}), bf16[4,64,2048]{2,1,0:T(8,128)(2,1)}, u32[]{:S(2)}, u32[]{:S(2)}) async-start(bf16[4,64,2048]{2,1,0:T(8,128)(2,1)} %broadcast_in_dim.24), calls=%async_computation | async-start | bytes 2097152 | tf_op jit(solution)/shard_map/all_to_all | solution.py:12
  21.5 14.8 %all-to-all-done = bf16[4,64,2048]{2,1,0:T(8,128)(2,1)} async-done(((bf16[4,64,2048]{2,1,0:T(8,128)(2,1)}), bf16[4,64,2048]{2,1,0:T(8,128)(2,1)}, u32[]{:S(2)}, u32[]{:S(2)}) %all-to-all-start) | async-done | bytes 1048608 | tf_op jit(solution)/shard_map/all_to_all | solution.py:12
  36.3 1.4 convert_reduce_fusion
  37.7 1.1 fusion.59
  38.8 1.2 multiply_reduce_fusion.1
  40.0 1.1 fusion.23
  41.2 0.7 copy-done.3
  41.8 1.5 convolution_convert_fusion.1
  43.3 2.3 %reshape.112 = bf16[32,2,4,2048]{3,2,1,0:T(4,128)(2,1)} reshape(bf16[256,2048]{1,0:T(8,128)(2,1)} %convolution_convert_fusion.1) | data formatting | bytes 2097152 | tf_op jit(solution)/shard_map/reshape | solution.py:170
  45.6 1.0 constant_dynamic-slice_fusion
  46.6 46.5 %all_to_all.25 = bf16[32,2,4,512]{3,2,1,0:T(4,128)(2,1)S(1)} all-to-all(bf16[32,2,4,512]{3,2,1,0:T(4,128)(2,1)S(1)} %constant_dynamic-slice_fusion), channel_id=1, replica_groups=mesh['grp'=2,'ep'=32,'tp'=4] {'ep'}, dimensions={0} | all-to-all | bytes 524288 | tf_op jit(solution)/shard_map/all_to_all | solution.py:176
  93.4 18.0 %all_to_all.26 = bf16[4,32,2,4,512]{4,1,3,2,0:T(8,128)(2,1)S(1)} all-to-all(bf16[4,32,2,4,512]{4,1,3,2,0:T(8,128)(2,1)S(1)} %broadcast_in_dim.34), channel_id=1, replica_groups=mesh['grp'=2,'ep'=32,'tp'=4] {'tp'}, dimensions={0} | all-to-all | bytes 2097152 | tf_op jit(solution)/shard_map/all_to_all | solution.py:12
  111.6 1.0 copy-done.1
  112.6 1.2 fusion.7
  113.7 3.8 %convolution_convert_fusion = bf16[2,32,4,2048]{3,1,2,0:T(8,128)(2,1)} fusion(bf16[2,256,2048]{2,1,0:T(8,128)(2,1)S(1)} %copy-done, bf16[32,2,4,2048]{3,0,2,1:T(8,128)(2,1)} %bitcast.88, bf16[2,2048,256]{2,1,0:T(8,128)(2,1)} %param.33, f32[32,2,4,256]{3,0,2,1:T(8,128)} %fusion.7), kind=kOutput, calls=%fused_computation | convolution fusion | flops 537788416 | bytes 6553600 | tf_op jit(solution)/shard_map/njcf,jfd->njcd/dot_general | solution.py:182
  117.5 1.4 copy.96
  118.8 17.5 %all_to_all.27 = bf16[4,32,2,4,512]{4,1,3,2,0:T(8,128)(2,1)} all-to-all(bf16[4,32,2,4,512]{4,1,3,2,0:T(8,128)(2,1)S(1)} %bitcast.92), channel_id=1, replica_groups=mesh['grp'=2,'ep'=32,'tp'=4] {'tp'}, dimensions={0} | all-to-all | bytes 2097152 | tf_op jit(solution)/shard_map/all_to_all | solution.py:38
  136.3 2.2 %reduce_sum.130 = bf16[32,2,4,512]{3,0,2,1:T(8,128)(2,1)} reduce(bf16[4,32,2,4,512]{4,1,3,2,0:T(8,128)(2,1)} %all_to_all.27, bf16[]{:T(256)} %constant.58.clone.1), dimensions={0}, to_apply=%region_12.13 | reduce | flops 393216 | bytes 1310722 | tf_op jit(solution)/shard_map/reduce_sum | solution.py:39
  138.5 1.2 copy.80
  139.7 26.5 %all_to_all.28 = bf16[32,2,4,512]{3,2,1,0:T(4,128)(2,1)} all-to-all(bf16[32,2,4,512]{3,2,1,0:T(4,128)(2,1)S(1)} %copy.80), channel_id=1, replica_groups=mesh['grp'=2,'ep'=32,'tp'=4] {'ep'}, dimensions={0} | all-to-all | bytes 524288 | tf_op jit(solution)/shard_map/all_to_all | solution.py:188
  166.2 1.7 all_gather_reshape.3
  168.0 1.5 pad_maximum_fusion
  169.5 1.3 copy.82
  171.7 16.1 %all-gather.2.cloned.1.call-done = bf16[4,256,512]{2,1,0:T(8,128)(2,1)} async-done(((bf16[1,256,512]{2,1,0:T(8,128)(2,1)}), bf16[4,256,512]{2,1,0:T(8,128)(2,1)}) %all-gather.2.cloned.1.call-update) | async-done | bytes 1048592 | tf_op jit(solution)/shard_map/all_gather | solution.py:192
  187.8 2.3 %copy.81 = bf16[4,256,512]{1,2,0:T(8,128)(2,1)} copy(bf16[4,256,512]{2,1,0:T(8,128)(2,1)} %all-gather.2.cloned.1.call-done) | data formatting | bytes 2097152 | tf_op jit(solution)/shard_map/all_gather | solution.py:192
  190.0 1.8 fusion.62
  192.1 0.8 multiply_convert_fusion
  (65 shorter events, 4.2 us)
Async XLA Ops:
  7.2 106.6 %copy-start = (bf16[2,256,2048]{2,1,0:T(8,128)(2,1)S(1)}, bf16[2,256,2048]{2,1,0:T(8,128)(2,1)}, u32[]{:S(2)}) copy-start(bf16[2,256,2048]{2,1,0:T(8,128)(2,1)} %param.34) | copy-start | bytes 6291460
  7.2 2.9 %copy-start.5 = (f32[64,24,128]{2,1,0:T(8,128)S(1)}, f32[64,24,128]{2,1,0:T(8,128)}, u32[]{:S(2)}) copy-start(f32[64,24,128]{2,1,0:T(8,128)} %param.19) | copy-start | bytes 2359300
  9.9 0.7 copy-start.14
  9.9 0.7 copy-start.15
  9.9 0.9 copy-start.9
  10.9 1.9 copy-start.17
  10.9 2.0 copy-start.8
  12.9 2.0 copy-start.7
  15.3 5.8 %copy-start.13 = (s32[64,2]{0,1:T(2,128)S(1)}, s32[64,2]{0,1:T(2,128)}, u32[]{:S(2)}) copy-start(s32[64,2]{0,1:T(2,128)} %param.20) | copy-start | bytes 1540
  16.4 19.8 %all-to-all-start = ((bf16[4,64,2048]{2,1,0:T(8,128)(2,1)}), bf16[4,64,2048]{2,1,0:T(8,128)(2,1)}, u32[]{:S(2)}, u32[]{:S(2)}) async-start(bf16[4,64,2048]{2,1,0:T(8,128)(2,1)} %broadcast_in_dim.24), calls=%async_computation | async-start | bytes 2097152 | tf_op jit(solution)/shard_map/all_to_all | solution.py:12
  21.0 19.0 %copy-start.11 = (f32[2048]{0:T(1024)S(1)}, f32[2048]{0:T(1024)}, u32[]{:S(2)}) copy-start(f32[2048]{0:T(1024)} %param.29) | copy-start | bytes 24580
  21.0 166.8 %all-gather.2.cloned.1.call-start = ((), (), s32[]{:S(2)}) async-start(), calls=%async_computation.5 | async-start | bytes 1310720 | tf_op jit(solution)/shard_map/all_gather | solution.py:192
  41.1 0.7 copy-start.3
  93.4 19.2 %copy-start.6 = (bf16[2,2048,256]{2,1,0:T(8,128)(2,1)S(1)}, bf16[2,2048,256]{2,1,0:T(8,128)(2,1)}, u32[]{:S(2)}) copy-start(bf16[2,2048,256]{2,1,0:T(8,128)(2,1)} %param.32) | copy-start | bytes 6291460
  111.6 1.0 copy-start.1
  168.0 2.9 %copy-start.4 = (bf16[64,2048]{1,0:T(8,128)(2,1)S(1)}, bf16[64,2048]{1,0:T(8,128)(2,1)}, u32[]{:S(2)}) copy-start(bf16[64,2048]{1,0:T(8,128)(2,1)} %copy-done.3) | copy-start | bytes 786436
  168.0 2.9 %copy-start.10 = (bf16[2048,64]{0,1:T(8,128)(2,1)S(1)}, bf16[2048,64]{0,1:T(8,128)(2,1)}, u32[]{:S(2)}) copy-start(bf16[2048,64]{0,1:T(8,128)(2,1)} %param.31) | copy-start | bytes 786436
  168.0 3.3 %copy-start.12 = (bf16[2048,4]{0,1:T(4,128)(2,1)S(1)}, bf16[2048,4]{0,1:T(4,128)(2,1)}, u32[]{:S(2)}) copy-start(bf16[2048,4]{0,1:T(4,128)(2,1)} %param.30) | copy-start | bytes 49156
  169.5 20.6 %copy-start.2 = (bf16[64,2048]{1,0:T(8,128)(2,1)S(1)}, bf16[64,2048]{1,0:T(8,128)(2,1)}, u32[]{:S(2)}) copy-start(bf16[64,2048]{1,0:T(8,128)(2,1)} %param.18) | copy-start | bytes 786436
  171.6 20.4 %copy-start.16 = (f32[2048]{0:T(1024)S(1)}, f32[2048]{0:T(1024)}, u32[]{:S(2)}) copy-start(f32[2048]{0:T(1024)} %param.35) | copy-start | bytes 24580
Sparse Core Ops, SparseCore 0:
  168.1 19.6 all-gather.1
